TPU v7x, 32 devices: a whole 2x2x4 slice. The times are simulated.
32 devices in a mesh: gr: 2 (over x), sp: 8 (over z, y), tp: 2 (over core).
Axes of the slice: x: 2, y: 2, z: 4, core: 2. Of those that a mesh axis runs over, the one named last changes fastest.
Arguments:
- tokens: bfloat16 [8, 1024, 4096], P('gr', 'sp'), parts along dimension 0, may hold values from -6 to 6
- key_weight: bfloat16 [4096, 2048], P('sp', 'tp'), may hold values from -0.09375 to 0.09375
- value_weight: bfloat16 [4096, 2048], P('sp', 'tp'), may hold values from -0.09375 to 0.09375
- log_decay: float32 [32, 8, 1024], P('tp', 'gr', 'sp'), parts along dimension 1, may hold values from -1 to 0, as said below
- new_query: bfloat16 [8, 2048], P('gr', 'tp'), parts along dimension 0, may hold values from -6 to 6
- new_key: bfloat16 [8, 2048], P('gr', 'tp'), parts along dimension 0, may hold values from -24 to 24
- new_value: bfloat16 [8, 2048], P('gr', 'tp'), parts along dimension 0, may hold values from -6 to 6
- step_decay: float32 [32, 8], P('tp', 'gr'), parts along dimension 1, may hold values from -1.5 to -0.05
- norm_gain: float32 [2048], P('tp'), may hold values from 0.1 to 1.9
Outputs:
- state_cache: float32 [512, 32, 64], P('gr', 'tp'), parts along dimension 0
- first_read: bfloat16 [8, 2048], P('gr', 'tp'), parts along dimension 0
There are 2 independent parts, one for each index of `gr`. A program takes and returns all parts, laid end to end along the dimension named above; an argument that names none is the same for every part. Nothing has to cross between parts.
Inputs may be any that keep to these rules, and one draw needn't show every extreme that they name: `log_decay`: every entry is at most zero.
All inputs are finite; a program needn't handle non-finite values.
Results may differ from a plain program's by a relative error of at most 0.0053.
Values may be sent and summed in bfloat16 or wider, within the bound.
A program may use at most 64 MiB of HBM per device.

v0:
```python
import jax
import jax.numpy as jnp
from jax import lax
from jax.sharding import PartitionSpec as P

HEAD_DIM = 64


def entering(x, axis, combine, identity):
    devices, mine = (lax.axis_size(axis), lax.axis_index(axis))
    everything = lax.all_gather(x, axis)
    start = jnp.broadcast_to(jnp.asarray(identity, x.dtype), x.shape)

    def lap(k, before):
        at = devices - 1 - k
        reached = at > mine
        new = combine(before, everything[at])
        return jnp.where(reached, new, before)

    return lax.fori_loop(0, devices, lap, start)


def rotate_half(values, positions):
    half = values.shape[-1] // 2
    inverse = 10000.0 ** (-jnp.arange(half, dtype=jnp.float32) * (2.0 / values.shape[-1]))
    angles = positions[..., None] * inverse
    cosine = jnp.cos(angles)
    sine = jnp.sin(angles)
    first, second = (values[..., :half], values[..., half:])
    return jnp.concatenate(
        [first * cosine - second * sine, second * cosine + first * sine], axis=-1
    )


def add_totals(earlier, later):
    return earlier + later


def shards(
    tokens,
    key_weight,
    value_weight,
    log_decay,
    new_query,
    new_key,
    new_value,
    step_decay,
    norm_gain,
):
    seqs, span, width = tokens.shape
    heads_here = key_weight.shape[1] // HEAD_DIM
    token_rows = tokens.reshape(seqs * span, width)
    whole_keys, whole_values = (
        lax.all_gather(key_weight, "sp", axis=0, tiled=True),
        lax.all_gather(value_weight, "sp", axis=0, tiled=True),
    )
    key_sum = jnp.dot(token_rows, whole_keys, preferred_element_type=jnp.float32)
    value_sum = jnp.dot(token_rows, whole_values, preferred_element_type=jnp.float32)
    key_vectors = (
        lax.optimization_barrier(key_sum.astype(jnp.bfloat16))
        .astype(jnp.float32)
        .reshape(seqs, span, heads_here, HEAD_DIM)
    )
    values = (
        lax.optimization_barrier(value_sum.astype(jnp.bfloat16))
        .astype(jnp.float32)
        .reshape(seqs, span, heads_here, HEAD_DIM)
    )
    devices = lax.axis_size("sp")
    offset = lax.axis_index("sp") * span
    positions = (offset + jnp.arange(span, dtype=jnp.int32)).astype(jnp.float32)
    rkeys = rotate_half(key_vectors, positions[None, :, None]) * HEAD_DIM ** (-0.5)
    totals = jnp.sum(log_decay, axis=-1)
    later_sum = entering(totals, "sp", add_totals, jnp.zeros_like(totals))
    weight = jnp.exp(totals[:, :, None] - jnp.cumsum(log_decay, axis=-1) + later_sum[:, :, None])
    weighted = rkeys * jnp.transpose(weight, (1, 2, 0))[:, :, :, None]
    term = jnp.einsum("stha,sthb->sahb", weighted, values, precision=lax.Precision.HIGHEST)
    term = term.reshape(seqs * HEAD_DIM, heads_here, HEAD_DIM)
    end_pos = jnp.full((seqs, heads_here), float(span * devices), jnp.float32)
    query = rotate_half(new_query.astype(jnp.float32).reshape(seqs, heads_here, HEAD_DIM), end_pos)
    key_new = rotate_half(
        new_key.astype(jnp.float32).reshape(seqs, heads_here, HEAD_DIM), end_pos
    ) * HEAD_DIM ** (-0.5)
    value_new = new_value.astype(jnp.float32).reshape(seqs, heads_here, HEAD_DIM)
    decay_all = jnp.repeat(jnp.exp(step_decay).T, HEAD_DIM, axis=0)
    key_all = jnp.transpose(key_new, (0, 2, 1)).reshape(seqs * HEAD_DIM, heads_here)
    value_all = jnp.repeat(value_new, HEAD_DIM, axis=0)
    summed = lax.psum(term, "sp")
    state_cache = decay_all[:, :, None] * summed + key_all[:, :, None] * value_all
    state_seq = state_cache.reshape(seqs, HEAD_DIM, heads_here, HEAD_DIM)
    raw = jnp.einsum("sha,sahb->shb", query, state_seq, precision=lax.Precision.HIGHEST)
    center = jnp.mean(raw, axis=-1, keepdims=True)
    spread = jnp.mean(jnp.square(raw - center), axis=-1, keepdims=True)
    normed = (raw - center) * lax.rsqrt(spread + 1e-06) * norm_gain.reshape(heads_here, HEAD_DIM)
    first_read = normed.reshape(seqs, heads_here * HEAD_DIM).astype(jnp.bfloat16)
    return (state_cache, first_read)


def solution(mesh):
    placed = (
        P("gr", "sp", None),
        P("sp", "tp"),
        P("sp", "tp"),
        P("tp", "gr", "sp"),
        P("gr", "tp"),
        P("gr", "tp"),
        P("gr", "tp"),
        P("tp", "gr"),
        P("tp"),
    )
    return jax.shard_map(
        shards,
        mesh=mesh,
        in_specs=placed,
        out_specs=(P("gr", "tp", None), P("gr", "tp")),
        check_vma=False,
    )
```

profile of v0, /device:TPU:0, one launch (start us, length us, event | category | flops | bytes accessed | tf_op | source)
XLA Modules:
  0.0 378.3 jit_solution(3645071348651051041)
XLA Ops:
  7.2 0.7 all-gather.7.cloned.1.call-update
  8.0 0.7 all-gather.5.cloned.1.call-update
  9.0 1.1 reduce_window_sum.13
  10.1 28.8 %all-gather.1 = f32[8,16,4]{1,2,0:T(4,128)S(1)} all-gather(f32[1,16,4]{1,2,0:T(4,128)S(1)} %bitcast.52), channel_id=2, replica_groups=mesh['gr'=2,'sp'=8,'tp'=2] {'sp'}, dimensions={0}, use_global_device_ids=true | all-gather | bytes 2304 | tf_op jit(solution)/shard_map/all_gather | solution.py:11
  38.9 0.3 while.16
  39.5 98.0 %all-gather.7.cloned.1.call-done = bf16[4096,1024]{1,0:T(8,128)(2,1)} async-done(((bf16[512,1024]{1,0:T(8,128)(2,1)}), bf16[4096,1024]{1,0:T(8,128)(2,1)}) %all-gather.7.cloned.1.call-update) | async-done | bytes 8388624 | tf_op jit(solution)/shard_map/all_gather | solution.py:54
  137.5 9.1 %convolution_convert_fusion = bf16[512,1024]{1,0:T(8,128)(2,1)S(1)} fusion(bf16[512,4096]{1,0:T(8,128)(2,1)} %bitcast.53, bf16[4096,1024]{1,0:T(8,128)(2,1)} %all-gather.7.cloned.1.call-done), kind=kOutput, calls=%fused_computation.8 | convolution fusion | flops 4295491584 | bytes 13631488 | tf_op jit(solution)/shard_map/dot_general | solution.py:57
  146.6 115.7 %all-gather.5.cloned.1.call-done = bf16[4096,1024]{1,0:T(8,128)(2,1)} async-done(((bf16[512,1024]{1,0:T(8,128)(2,1)}), bf16[4096,1024]{1,0:T(8,128)(2,1)}) %all-gather.5.cloned.1.call-update) | async-done | bytes 8388624 | tf_op jit(solution)/shard_map/all_gather | solution.py:55
  262.3 10.1 %convolution_convert_fusion.1 = bf16[512,1024]{1,0:T(8,128)(2,1)} fusion(bf16[512,4096]{1,0:T(8,128)(2,1)} %bitcast.54, bf16[4096,1024]{1,0:T(8,128)(2,1)} %all-gather.5.cloned.1.call-done), kind=kOutput, calls=%fused_computation.9 | convolution fusion | flops 4295491584 | bytes 13631488 | tf_op jit(solution)/shard_map/dot_general | solution.py:58
  272.4 2.9 reshape.171
  275.4 1.7 copy.30
  277.0 2.9 reshape.158
  279.9 2.1 multiply_subtract_fusion
  282.1 0.6 maximum_multiply_fusion
  282.7 2.1 fusion.5
  284.7 1.4 copy.37
  286.2 2.1 reshape.148
  289.4 1.2 broadcast_in_dim.8
  290.6 1.1 reshape.153
  291.9 73.2 %all-reduce.2.cloned.1.call-done = f32[256,16,64]{0,2,1:T(8,128)} async-done(((f32[256,16,64]{0,2,1:T(8,128)}), f32[256,16,64]{0,2,1:T(8,128)}) %all-reduce.2.cloned.1.call-update) | async-done | bytes 1048592 | tf_op jit(solution)/shard_map/psum | solution.py:88
  365.0 1.4 multiply_add_fusion
  366.4 0.9 reshape.156
  367.3 3.4 fusion.2
  371.1 0.7 convert_element_type.28
  (55 shorter events, 2.2 us)
Async XLA Ops:
  7.2 1.6 copy-start.1
  7.2 130.3 %all-gather.7.cloned.1.call-start = ((), (), s32[]{:S(2)}) async-start(), calls=%async_computation.1 | async-start | bytes 9437184 | tf_op jit(solution)/shard_map/all_gather | solution.py:54
  7.9 254.4 %all-gather.5.cloned.1.call-start = ((), (), s32[]{:S(2)}) async-start(), calls=%async_computation | async-start | bytes 9437184 | tf_op jit(solution)/shard_map/all_gather | solution.py:55
  8.7 356.3 %all-reduce.2.cloned.1.call-start = ((), (), s32[]{:S(2)}) async-start(), calls=%async_computation.2 | async-start | bytes 2097152 | tf_op jit(solution)/shard_map/psum | solution.py:88
  286.2 2.2 copy-start.6
  286.2 2.3 copy-start.5
  286.2 2.5 copy-start.3
  286.2 2.6 copy-start.4
  286.2 3.0 copy-start.2
  366.4 4.3 %copy-start = (f32[256,16,64]{0,2,1:T(8,128)}, f32[256,16,64]{0,2,1:T(8,128)S(1)}, u32[]{:S(2)}) copy-start(f32[256,16,64]{0,2,1:T(8,128)S(1)} %multiply_add_fusion) | copy-start | bytes 3145732
Sparse Core Ops, SparseCore 0:
  10.1 127.3 all-gather.6
  139.6 122.6 all-gather.4
  288.5 76.4 all-reduce.1
where the time goes:
time: 379 us; the launch traced here: 378 us
  waiting for transfers between devices  288 us (76%)
  blocking collectives  28.8 us (8%)
  matrix products  24.7 us (7%)
  local copies, waits for them, and re-layouts  16 us (4%)
  between operations  14 us (4%)
  other arithmetic  6.37 us (2%)
    all_gather x1, waiting for transfers between devices, shards(): lax.all_gather(value_weight, 'sp', axis=0, tiled=True)  116 us
    all_gather x1, waiting for transfers between devices, shards(): lax.all_gather(key_weight, 'sp', axis=0, tiled=True)  98 us
    psum x1, waiting for transfers between devices, shards(): summed = lax.psum(term, 'sp')  73.2 us
    all_gather x1, blocking collectives, entering(): everything = lax.all_gather(x, axis)  28.8 us
    dot_general x1, matrix products, shards(): jnp.dot(token_rows, whole_values, preferred_element_type=jnp.float32)  10.1 us
    dot_general x1, matrix products, shards(): jnp.dot(token_rows, whole_keys, preferred_element_type=jnp.float32)  9.14 us
  transfers between devices with their start and end apart: 3, of which 3 were waited for; matrix products, arithmetic and copies ran while one was open for 4% of the time, Pallas kernels for 0%

commit v1 on v0

--- a/solution.py
+++ b/solution.py
@@ -85,7 +85,9 @@
     decay_all = jnp.repeat(jnp.exp(step_decay).T, HEAD_DIM, axis=0)
     key_all = jnp.transpose(key_new, (0, 2, 1)).reshape(seqs * HEAD_DIM, heads_here)
     value_all = jnp.repeat(value_new, HEAD_DIM, axis=0)
-    summed = lax.psum(term, "sp")
+    summed = term
+    for hop in (1, 2, 4):
+        summed = summed + lax.ppermute(summed, "sp", [(dev, dev ^ hop) for dev in range(8)])
     state_cache = decay_all[:, :, None] * summed + key_all[:, :, None] * value_all
     state_seq = state_cache.reshape(seqs, HEAD_DIM, heads_here, HEAD_DIM)
     raw = jnp.einsum("sha,sahb->shb", query, state_seq, precision=lax.Precision.HIGHEST)

time: 379 us -> 396 us (1.045)
  waiting for transfers between devices: 288 us -> 300 us
    ppermute x0 -> x3, waiting for transfers between devices: none -> 84.8 us  [shards(): lax.ppermute(summed, 'sp', [(dev, dev ^ hop) for dev in range(8)])]
    psum x1 -> x0, waiting for transfers between devices: 73.2 us -> none  [shards(): summed = lax.psum(term, 'sp')]
  transfers between devices with their start and end apart: 3 -> 5, of which waited for: 3 -> 5; matrix products, arithmetic and copies ran while one was open for 4% -> 4% of each run, Pallas kernels for 0% -> 0%
where the time goes in v1:
time: 396 us; the launch traced here: 395 us
  waiting for transfers between devices  300 us (76%)
  blocking collectives  28.8 us (7%)
  matrix products  24.7 us (6%)
  local copies, waits for them, and re-layouts  17.7 us (4%)
  between operations  14.3 us (4%)
  other arithmetic  7.11 us (2%)
    all_gather x1, waiting for transfers between devices, shards(): lax.all_gather(value_weight, 'sp', axis=0, tiled=True)  116 us
    all_gather x1, waiting for transfers between devices, shards(): lax.all_gather(key_weight, 'sp', axis=0, tiled=True)  98 us
    ppermute x3, waiting for transfers between devices, shards(): lax.ppermute(summed, 'sp', [(dev, dev ^ hop) for dev in range(8)])  84.8 us
    all_gather x1, blocking collectives, entering(): everything = lax.all_gather(x, axis)  28.8 us
    dot_general x1, matrix products, shards(): jnp.dot(token_rows, whole_values, preferred_element_type=jnp.float32)  10.1 us
    dot_general x1, matrix products, shards(): jnp.dot(token_rows, whole_keys, preferred_element_type=jnp.float32)  9.14 us
  transfers between devices with their start and end apart: 5, of which 5 were waited for; matrix products, arithmetic and copies ran while one was open for 4% of the time, Pallas kernels for 0%

profile of v1, /device:TPU:0, one launch (start us, length us, event | category | flops | bytes accessed | tf_op | source)
XLA Modules:
  0.0 395.3 jit_solution(8710993121616879138)
XLA Ops:
  8.0 0.7 all-gather.5.cloned.1.call-update
  9.0 1.1 reduce_window_sum.13
  10.1 28.8 %all-gather.1 = f32[8,16,4]{1,2,0:T(4,128)S(1)} all-gather(f32[1,16,4]{1,2,0:T(4,128)S(1)} %bitcast.52), channel_id=2, replica_groups=mesh['gr'=2,'sp'=8,'tp'=2] {'sp'}, dimensions={0}, use_global_device_ids=true | all-gather | bytes 2304 | tf_op jit(solution)/shard_map/all_gather | solution.py:11
  39.5 98.0 %all-gather.7.cloned.1.call-done = bf16[4096,1024]{1,0:T(8,128)(2,1)} async-done(((bf16[512,1024]{1,0:T(8,128)(2,1)}), bf16[4096,1024]{1,0:T(8,128)(2,1)}) %all-gather.7.cloned.1.call-update) | async-done | bytes 8388624 | tf_op jit(solution)/shard_map/all_gather | solution.py:54
  137.4 9.1 %convolution_convert_fusion = bf16[512,1024]{1,0:T(8,128)(2,1)S(1)} fusion(bf16[512,4096]{1,0:T(8,128)(2,1)} %bitcast.53, bf16[4096,1024]{1,0:T(8,128)(2,1)} %all-gather.7.cloned.1.call-done), kind=kOutput, calls=%fused_computation.8 | convolution fusion | flops 4295491584 | bytes 13631488 | tf_op jit(solution)/shard_map/dot_general | solution.py:57
  146.6 115.7 %all-gather.5.cloned.1.call-done = bf16[4096,1024]{1,0:T(8,128)(2,1)} async-done(((bf16[512,1024]{1,0:T(8,128)(2,1)}), bf16[4096,1024]{1,0:T(8,128)(2,1)}) %all-gather.5.cloned.1.call-update) | async-done | bytes 8388624 | tf_op jit(solution)/shard_map/all_gather | solution.py:55
  262.3 10.1 %convolution_convert_fusion.1 = bf16[512,1024]{1,0:T(8,128)(2,1)} fusion(bf16[512,4096]{1,0:T(8,128)(2,1)} %bitcast.54, bf16[4096,1024]{1,0:T(8,128)(2,1)} %all-gather.5.cloned.1.call-done), kind=kOutput, calls=%fused_computation.9 | convolution fusion | flops 4295491584 | bytes 13631488 | tf_op jit(solution)/shard_map/dot_general | solution.py:58
  272.4 2.9 reshape.171
  275.3 1.6 copy.30
  277.0 2.9 reshape.158
  279.9 2.1 multiply_subtract_fusion
  282.6 2.1 fusion.5
  284.7 1.4 copy.37
  286.1 1.1 reshape.148
  287.8 23.6 %collective-permute-done = f32[256,16,64]{0,2,1:T(8,128)S(1)} collective-permute-done((f32[256,16,64]{0,2,1:T(8,128)S(1)}, f32[256,16,64]{0,2,1:T(8,128)S(1)}, u32[]{:S(2)}, u32[]{:S(2)}) %collective-permute-start) | collective-permute-done | bytes 1048608 | tf_op jit(solution)/shard_map/ppermute | solution.py:90
  311.8 23.3 %collective-permute-done.1 = f32[256,16,64]{0,2,1:T(8,128)S(1)} collective-permute-done((f32[256,16,64]{0,2,1:T(8,128)S(1)}, f32[256,16,64]{0,2,1:T(8,128)S(1)}, u32[]{:S(2)}, u32[]{:S(2)}) %collective-permute-start.1) | collective-permute-done | bytes 1048608 | tf_op jit(solution)/shard_map/ppermute | solution.py:90
  335.3 1.9 collective-permute-start.2
  338.0 1.0 copy.45
  339.0 2.2 broadcast_in_dim.8
  341.2 2.1 reshape.153
  343.4 37.9 %collective-permute-done.2 = f32[256,16,64]{0,2,1:T(8,128)} collective-permute-done((f32[256,16,64]{0,2,1:T(8,128)S(1)}, f32[256,16,64]{0,2,1:T(8,128)}, u32[]{:S(2)}, u32[]{:S(2)}) %collective-permute-start.2) | collective-permute-done | bytes 1048608 | tf_op jit(solution)/shard_map/ppermute | solution.py:90
  381.3 1.8 multiply_add_fusion
  383.1 0.9 reshape.156
  384.0 3.4 fusion.2
  (60 shorter events, 5.3 us)
Async XLA Ops:
  7.2 1.5 copy-start.1
  7.2 130.3 %all-gather.7.cloned.1.call-start = ((), (), s32[]{:S(2)}) async-start(), calls=%async_computation.1 | async-start | bytes 9437184 | tf_op jit(solution)/shard_map/all_gather | solution.py:54
  7.9 254.4 %all-gather.5.cloned.1.call-start = ((), (), s32[]{:S(2)}) async-start(), calls=%async_computation | async-start | bytes 9437184 | tf_op jit(solution)/shard_map/all_gather | solution.py:55
  287.2 24.2 %collective-permute-start = (f32[256,16,64]{0,2,1:T(8,128)S(1)}, f32[256,16,64]{0,2,1:T(8,128)S(1)}, u32[]{:S(2)}, u32[]{:S(2)}) collective-permute-start(f32[256,16,64]{0,2,1:T(8,128)S(1)} %reshape.148), channel_id=1, source_target_pairs={{0,2},{2,0},{4,6},{6,4},{8,10},{10,8},{12,14},{14,12},{1,3},{3,1},... | collective-permute-start | bytes 3145736 | tf_op jit(solution)/shard_map/ppermute | solution.py:90
  311.6 25.5 %copy-start.6 = (f32[16,4]{0,1:T(4,128)S(1)}, f32[16,4]{0,1:T(4,128)}, u32[]{:S(2)}) copy-start(f32[16,4]{0,1:T(4,128)} %param.18) | copy-start | bytes 772
  311.6 25.6 %copy-start.5 = (f32[1024]{0:T(1024)S(1)}, f32[1024]{0:T(1024)}, u32[]{:S(2)}) copy-start(f32[1024]{0:T(1024)} %param.19) | copy-start | bytes 12292
  311.7 25.8 %copy-start.3 = (bf16[4,1024]{1,0:T(4,128)(2,1)S(1)}, bf16[4,1024]{1,0:T(4,128)(2,1)}, u32[]{:S(2)}) copy-start(bf16[4,1024]{1,0:T(4,128)(2,1)} %param.15) | copy-start | bytes 24580
  311.7 25.9 %copy-start.4 = (bf16[4,1024]{1,0:T(4,128)(2,1)S(1)}, bf16[4,1024]{1,0:T(4,128)(2,1)}, u32[]{:S(2)}) copy-start(bf16[4,1024]{1,0:T(4,128)(2,1)} %param.16) | copy-start | bytes 24580
  311.7 26.3 %copy-start.2 = (bf16[4,1024]{1,0:T(4,128)(2,1)S(1)}, bf16[4,1024]{1,0:T(4,128)(2,1)}, u32[]{:S(2)}) copy-start(bf16[4,1024]{1,0:T(4,128)(2,1)} %param.17) | copy-start | bytes 24580
  311.7 23.4 %collective-permute-start.1 = (f32[256,16,64]{0,2,1:T(8,128)S(1)}, f32[256,16,64]{0,2,1:T(8,128)S(1)}, u32[]{:S(2)}, u32[]{:S(2)}) collective-permute-start(f32[256,16,64]{0,2,1:T(8,128)S(1)} %add.99), channel_id=1, source_target_pairs={{0,4},{2,6},{4,0},{6,2},{8,12},{10,14},{12,8},{14,10},{1,5},{3,7},... | collective-permute-start | bytes 3145736 | tf_op jit(solution)/shard_map/ppermute | solution.py:90
  335.3 46.0 %collective-permute-start.2 = (f32[256,16,64]{0,2,1:T(8,128)S(1)}, f32[256,16,64]{0,2,1:T(8,128)}, u32[]{:S(2)}, u32[]{:S(2)}) collective-permute-start(f32[256,16,64]{0,2,1:T(8,128)S(1)} %add.100), channel_id=1, source_target_pairs={{0,8},{2,10},{4,12},{6,14},{8,0},{10,2},{12,4},{14,6},{1,9},{3,11}... | collective-permute-start | bytes 3145736 | tf_op jit(solution)/shard_map/ppermute | solution.py:90
  383.1 4.3 %copy-start = (f32[256,16,64]{0,2,1:T(8,128)}, f32[256,16,64]{0,2,1:T(8,128)S(1)}, u32[]{:S(2)}) copy-start(f32[256,16,64]{0,2,1:T(8,128)S(1)} %multiply_add_fusion) | copy-start | bytes 3145732
Sparse Core Ops, SparseCore 0:
  10.1 127.2 all-gather.6
  139.6 122.6 all-gather.4
